TPU v7x, 32 devices: a whole 2x2x4 slice. The times are simulated.
32 devices in a mesh: sp: 8 (over z, y), tp: 4 (over x, core).
Axes of the slice: x: 2, y: 2, z: 4, core: 2. Of those that a mesh axis runs over, the one named last changes fastest.
Arguments:
- stream: bfloat16 [2048, 2048], P('sp'), may hold values from -6 to 6
- narrow_query_weight: bfloat16 [2048, 1024], P('sp', 'tp'), may hold values from -6 to 6
- wide_query_weight: bfloat16 [2048, 2048], P('sp', 'tp'), may hold values from -6 to 6
- value_rows_heads: bfloat16 [2048, 2, 1024], P('sp', None, 'tp'), may hold values from -6 to 6
- output_gate_logits: bfloat16 [2048, 2, 1024], P('sp', None, 'tp'), may hold values from -6 to 6
- narrow_forget_logits: bfloat16 [2, 2048, 1024], P(None, 'sp', 'tp'), may hold values from -6 to 6
- wide_forget_logits: bfloat16 [2, 2048, 2048], P(None, 'sp', 'tp'), may hold values from -6 to 6
- narrow_forget_headroom: float32 [2, 1024], P(None, 'tp'), may hold values from 0 to 0.08, as said below
- wide_forget_headroom: float32 [2, 2048], P(None, 'tp'), may hold values from 0 to 0.08, as said below
- extra_log_decay: float32 [2048, 2, 16], P('sp', None, 'tp'), may hold values from -1.4 to 0
- per_head_norm_gain: float32 [64], replicated, may hold values from 0.1 to 1.9
- mixer_output_weight: bfloat16 [2, 1024, 2048], replicated, may hold values from -0.125 to 0.125
- feedforward_norm_gain: float32 [2048], replicated, may hold values from 0.1 to 1.9
- expert_gate_matrix: bfloat16 [8, 2048, 4096], P('sp', None, 'tp'), may hold values from -0.125 to 0.125
- expert_up_matrix: bfloat16 [8, 2048, 4096], P('sp', None, 'tp'), may hold values from -0.125 to 0.125
- expert_down_matrix: bfloat16 [8, 4096, 2048], P('sp', 'tp'), may hold values from -0.09375 to 0.09375
- routes: int32 [2048, 2], P('sp'), may hold values from 0 to 7, all different within a row; in each aligned block of 64 rows (0 to 63, 64 to 127, ...) at most 32 rows name the same one
- router_scores_chosen: float32 [2048, 2], P('sp'), may hold values from -8 to 8
Outputs:
- result: bfloat16 [2048, 2048], P(('sp', 'tp'))
Inputs may be any that keep to these rules, and one draw needn't show every extreme that they name: `routes`: each row names 2 different experts; in each aligned block of 64 rows no expert is named by more than 32 rows. `narrow_forget_headroom`: positive. `wide_forget_headroom`: positive.
All inputs are finite; a program needn't handle non-finite values.
Results may differ from a plain program's by a relative error of at most 0.011.
Values may be sent and summed in bfloat16 or wider, within the bound.
A program may use at most 128 MiB of HBM per device.

v0:
```python
from functools import partial

import jax
import jax.numpy as jnp
from jax import lax
from jax.sharding import PartitionSpec as P

BLOCK = 64


EPS = 1e-06
TOP_PRECISION = lax.Precision.HIGHEST


def entering_2(x, axis, join, neutral, backward):
    count = lax.axis_size(axis)
    place = lax.axis_index(axis)
    ahead = count - 1 - place if backward else place
    gathered = jax.tree.map(
        lambda a, kind: lax.all_gather(a.astype(kind), axis),
        x,
        jax.tree.map(lambda a: jnp.bfloat16 if a.dtype == jnp.float32 else a.dtype, x),
    )
    state = jax.tree.map(lambda a, e: jnp.zeros_like(a) + jnp.asarray(e, a.dtype), x, neutral)

    def one(turn, state):
        source = count - 1 - turn if backward else turn
        return join(
            state,
            jax.tree.map(
                lambda a, own: lax.dynamic_index_in_dim(a, source, 0, False).astype(own.dtype),
                gathered,
                x,
            ),
        )

    return lax.fori_loop(0, ahead, one, state)


def to_blocks(source, length):
    token_rows, total_head_count, breadth = source.shape
    return source.reshape(token_rows // length, length, total_head_count, breadth).transpose(
        0, 2, 1, 3
    )


def from_blocks(source):
    blocks, total_head_count, length, breadth = source.shape
    return source.transpose(0, 2, 1, 3).reshape(blocks * length, total_head_count, breadth)


def block_sweep(query_rows, block_openings, values, inside, initial):
    ending = inside[:, :, -1:, :]
    query_within_block = query_rows * jnp.exp(inside)
    k_inside = block_openings * jnp.exp(-inside)
    key_block_ending = block_openings * jnp.exp(ending - inside)
    length = query_rows.shape[2]
    triangle = jnp.tril(jnp.ones((length, length), jnp.float32))
    scores = (
        jnp.einsum("nhtk,nhsk->nhts", query_within_block, k_inside, precision=TOP_PRECISION)
        * triangle
    )
    within = jnp.einsum("nhts,nhsv->nhtv", scores, values, precision=TOP_PRECISION)

    def advance(present_state, inputs):
        block_of_queries, block_opening_state, block_of_values, ending_block = inputs
        state_readout = jnp.einsum(
            "ifm,imo->ifo", block_of_queries, present_state, precision=TOP_PRECISION
        )
        expanded_state = jnp.einsum(
            "lbi,lbp->lip", block_opening_state, block_of_values, precision=TOP_PRECISION
        )
        return (
            present_state * jnp.exp(ending_block[:, 0, :])[:, :, None] + expanded_state,
            state_readout,
        )

    closing, carried = lax.scan(
        advance, initial, (query_within_block, key_block_ending, values, ending)
    )
    return (within + carried, closing)


def prepare_inputs(query_rows, forget_gate, forget_headroom, surge_amount, head_slice):
    token_rows, total_head_count = surge_amount.shape
    query_heads = jax.nn.silu(query_rows.astype(jnp.float32)).reshape(
        token_rows, total_head_count, -1
    )
    value_heads = head_slice.astype(jnp.float32).reshape(token_rows, total_head_count, -1)
    pre_forget = forget_gate.astype(jnp.float32).reshape(2, token_rows, total_head_count, -1)
    block_openings = jax.nn.sigmoid(-pre_forget) * forget_headroom.reshape(
        2, 1, total_head_count, -1
    )
    decay_logarithm = jnp.log1p(-block_openings) + surge_amount[None, :, :, None]
    return (query_heads, block_openings, value_heads, decay_logarithm)


def combine_states(earlier, later):
    return tuple(
        (
            (
                earlier_one[0] * later_one[0],
                earlier_one[1] * later_one[0][:, :, None] + later_one[1],
            )
            for earlier_one, later_one in zip(earlier, later)
        )
    )


def entering_states(parts, backward):
    identity = tuple(((jnp.ones_like(member[0]), jnp.zeros_like(member[1])) for member in parts))
    if backward:
        return entering_2(parts, "sp", combine_states, identity, True)
    return entering_2(parts, "sp", combine_states, identity, False)


def one_direction(groups, backward):
    blocked = []
    insides = []
    running_state = []
    totals = []
    for group in groups:
        group_members = tuple((to_blocks(member, BLOCK) for member in group))
        inside = jnp.cumsum(group_members[3], axis=2)
        endings = inside[:, :, -1:, :]
        blocked.append(group_members)
        insides.append(inside)
        running_state.append(jnp.cumsum(endings, axis=0) - endings + inside)
        totals.append(jnp.sum(endings[:, :, 0, :], axis=0))
    swept = []
    closing = []
    for token_position in range(len(blocked)):
        group_members = blocked[token_position]
        zero_state = jnp.zeros(
            (group_members[0].shape[1], group_members[0].shape[3], group_members[2].shape[3]),
            jnp.float32,
        )
        result_pair = block_sweep(
            group_members[0],
            group_members[1],
            group_members[2],
            insides[token_position],
            zero_state,
        )
        swept.append(result_pair[0])
        closing.append(result_pair[1])
    parts = tuple(((jnp.exp(sum_log), state_end) for sum_log, state_end in zip(totals, closing)))
    entering = entering_states(parts, backward)
    outputs = []
    for token_position in range(len(blocked)):
        group_members = blocked[token_position]
        incoming_state = entering[token_position][1]
        state_readout = jnp.einsum(
            "qrxa,rai->qrxi",
            group_members[0] * jnp.exp(running_state[token_position]),
            incoming_state,
            precision=TOP_PRECISION,
        )
        outputs.append(from_blocks(swept[token_position] + state_readout))
    return outputs


def slot_table(block_routes, experts, capacity):
    flattened = block_routes.reshape(-1)
    matches = (flattened[:, None] == jnp.arange(experts, dtype=jnp.int32)[None, :]).astype(
        jnp.int32
    )
    earlier = jnp.cumsum(matches, axis=0) - matches
    token_position = jnp.sum(earlier * matches, axis=1)
    return (flattened * capacity + token_position).reshape(block_routes.shape)


def dispatch(block_slots, block_rows, slot_count):
    picks = jnp.sum(
        (block_slots[:, :, None] == jnp.arange(slot_count, dtype=jnp.int32)).astype(jnp.bfloat16),
        axis=1,
    )
    return jnp.einsum("rs,rd->sd", picks, block_rows, preferred_element_type=jnp.float32).astype(
        jnp.bfloat16
    )


def local(
    stream,
    narrow_query_weight,
    wide_query_weight,
    value_rows_heads,
    output_gate_logits,
    narrow_forget_logits,
    wide_forget_logits,
    narrow_forget_headroom,
    wide_forget_headroom,
    extra_log_decay,
    per_head_norm_gain,
    mixer_output_weight,
    feedforward_norm_gain,
    expert_gate_matrix,
    expert_up_matrix,
    expert_down_matrix,
    routes,
    router_scores_chosen,
):
    token_rows = stream.shape[0]
    prepared = [
        prepare_inputs(
            narrow_query_weight,
            narrow_forget_logits,
            narrow_forget_headroom,
            extra_log_decay[:, 0],
            value_rows_heads[:, 0],
        ),
        prepare_inputs(
            wide_query_weight,
            wide_forget_logits,
            wide_forget_headroom,
            extra_log_decay[:, 1],
            value_rows_heads[:, 1],
        ),
    ]
    ahead = one_direction(
        [(group[0], group[1][0], group[2], group[3][0]) for group in prepared], False
    )
    behind = one_direction(
        [
            (
                jnp.flip(group[0], 0),
                jnp.flip(group[1][1], 0),
                jnp.flip(group[2], 0),
                jnp.flip(group[3][1], 0),
            )
            for group in prepared
        ],
        True,
    )
    mixed_groups = []
    for head_group_index in range(2):
        summed = ahead[head_group_index] + jnp.flip(behind[head_group_index], 0)
        scale = lax.rsqrt(jnp.mean(summed * summed, axis=-1, keepdims=True) + EPS)
        gate_heads = jax.nn.silu(
            output_gate_logits[:, head_group_index].astype(jnp.float32)
        ).reshape(summed.shape)
        mixed_groups.append(
            (summed * scale * per_head_norm_gain * gate_heads).reshape(token_rows, -1)
        )
    mixed = jnp.stack(mixed_groups, axis=1).astype(jnp.bfloat16)
    model_width = mixer_output_weight.shape[2]
    projected = jnp.einsum(
        "tgc,gcd->td",
        lax.all_gather(mixed, "tp", axis=2, tiled=True),
        mixer_output_weight,
        preferred_element_type=jnp.float32,
    )
    residual = stream.astype(jnp.float32) + projected
    norm_rows = (
        residual
        * lax.rsqrt(jnp.mean(residual * residual, axis=-1, keepdims=True) + EPS)
        * feedforward_norm_gain
    ).astype(jnp.bfloat16)
    group_count = lax.axis_size("tp")
    experts = lax.axis_size("sp")
    row_count = token_rows // group_count
    top_count = routes.shape[1]
    capacity = max(2, 2 * top_count * row_count // experts)
    slot_count = experts * capacity
    own_index = lax.axis_index("tp")
    slot_ids = jax.vmap(partial(slot_table, experts=experts, capacity=capacity))(
        routes.reshape(group_count, row_count, top_count)
    )
    grouped_rows = norm_rows.reshape(group_count, row_count, model_width)
    gate_weights = expert_gate_matrix[0]
    up_weights = expert_up_matrix[0]
    down_weights = expert_down_matrix[0]
    own_slots = lax.dynamic_index_in_dim(slot_ids, own_index, 0, keepdims=False)
    own_rows = lax.dynamic_index_in_dim(grouped_rows, own_index, 0, keepdims=False)
    own_buffer = dispatch(own_slots, own_rows, slot_count).reshape(experts, capacity, model_width)
    arrived = lax.all_gather(
        lax.all_to_all(own_buffer, "sp", split_axis=0, concat_axis=0, tiled=True)[None],
        "tp",
        axis=0,
        tiled=True,
    )
    gate_part = jnp.einsum(
        "...d,df->...f", arrived, gate_weights, preferred_element_type=jnp.float32
    )
    up_part = jnp.einsum("...d,df->...f", arrived, up_weights, preferred_element_type=jnp.float32)
    hidden = (jax.nn.silu(gate_part) * up_part).astype(jnp.bfloat16)
    sources = hidden.shape[1]
    count = hidden.shape[2]
    flattened = hidden.reshape(-1, hidden.shape[3])
    summed_rows = lax.psum_scatter(
        jnp.dot(flattened, down_weights, preferred_element_type=jnp.float32).astype(jnp.bfloat16),
        "tp",
        scatter_dimension=0,
        tiled=True,
    )
    returning = summed_rows.reshape(sources, count, -1)
    returned = lax.all_to_all(returning, "sp", split_axis=0, concat_axis=0, tiled=True)
    picked = returned.reshape(slot_count, model_width)[own_slots]
    own_logits = lax.dynamic_slice_in_dim(router_scores_chosen, own_index * row_count, row_count, 0)
    weights = jax.nn.sigmoid(own_logits - own_logits[:, ::-1])
    own_residual = lax.dynamic_slice_in_dim(residual, own_index * row_count, row_count, 0)
    mixed_out = jnp.sum(weights[:, :, None] * picked.astype(jnp.float32), axis=1)
    return (own_residual + mixed_out).astype(jnp.bfloat16)


def solution(mesh):
    placed = (
        P("sp", None),
        P("sp", "tp"),
        P("sp", "tp"),
        P("sp", None, "tp"),
        P("sp", None, "tp"),
        P(None, "sp", "tp"),
        P(None, "sp", "tp"),
        P(None, "tp"),
        P(None, "tp"),
        P("sp", None, "tp"),
        P(),
        P(),
        P(),
        P("sp", None, "tp"),
        P("sp", None, "tp"),
        P("sp", "tp", None),
        P("sp", None),
        P("sp", None),
    )
    return jax.shard_map(
        local, mesh=mesh, in_specs=placed, out_specs=P(("sp", "tp"), None), check_vma=False
    )
```

profile of v0, /device:TPU:0, one launch (start us, length us, event | category | flops | bytes accessed | tf_op | source)
XLA Modules:
  0.0 612.0 jit_solution(5396480994974336095)
XLA Ops:
  23.6 3.8 rev.40
  31.1 3.0 rev.42
  35.3 2.3 fusion.136
  39.8 2.2 bitcast_multiply_fusion.1
  42.9 19.9 %while.89 = (s32[]{:T(128)}, f32[4,128,64]{1,2,0:T(8,128)S(1)}, f32[4,4,64,64]{3,2,1,0:T(8,128)}, f32[4,4,1,128]{3,1,2,0:T(4,128)}, f32[4,4,64,128]{3,2,1,0:T(8,...) while((s32[]{:T(128)}, f32[4,128,64]{1,2,0:T(8,128)S(1)}, ...), condition=%wide.region_18.19_spmd.clone, body=%wide.region_17.18_spmd.clone.sunk | while | flops 50462720 | bytes 990832 | solution.py:78
  42.9 1.9 fusion.188
  47.9 1.9 fusion.188
  52.9 1.9 fusion.188
  57.8 1.9 fusion.188
  62.8 35.4 %all-gather.7 = bf16[32,128,64]{1,2,0:T(8,128)(2,1)} all-gather(bf16[4,128,64]{1,2,0:T(8,128)(2,1)S(1)} %convert_element_type.240), channel_id=9, replica_groups=mesh['sp'=8,'tp'=4] {'sp'}, dimensions={0}, use_global_device_ids=true | all-gather | bytes 589824 | tf_op jit(solution)/shard_map/all_gather | solution.py:20
  106.1 3.1 convolution_multiply_fusion
  109.1 2.9 convolution_multiply_fusion.2
  120.9 15.2 %while.88 = (s32[]{:T(128)}, f32[4,64,64]{2,1,0:T(8,128)S(1)}, f32[4,4,64,64]{3,2,1,0:T(8,128)}, f32[4,4,1,64]{3,1,2,0:T(4,128)}, f32[4,4,64,64]{3,2,1,0:T(8,128...) while((s32[]{:T(128)}, f32[4,64,64]{2,1,0:T(8,128)S(1)}, ...), condition=%wide.region_13.14_spmd.clone, body=%wide.region_12.13_spmd.clone.sunk | while | flops 25231364 | bytes 792684 | solution.py:78
  120.9 1.8 fusion.183
  124.7 1.8 fusion.183
  128.5 1.8 fusion.183
  136.2 33.2 %all-gather.5 = bf16[32,64,64]{2,1,0:T(8,128)(2,1)} all-gather(bf16[4,64,64]{2,1,0:T(8,128)(2,1)S(1)} %convert_element_type.235), channel_id=7, replica_groups=mesh['sp'=8,'tp'=4] {'sp'}, dimensions={0}, use_global_device_ids=true | all-gather | bytes 294912 | tf_op jit(solution)/shard_map/all_gather | solution.py:20
  170.0 21.5 %all-gather.12 = bf16[8,4,128]{2,1,0:T(4,128)(2,1)} all-gather(bf16[1,4,128]{2,1,0:T(4,128)(2,1)S(1)} %fusion.127), channel_id=8, replica_groups=mesh['sp'=8,'tp'=4] {'sp'}, dimensions={0}, use_global_device_ids=true | all-gather | bytes 9216 | tf_op jit(solution)/shard_map/all_gather | solution.py:20
  192.2 17.2 %all-gather.11 = bf16[8,4,64]{2,1,0:T(4,128)(2,1)} all-gather(bf16[1,4,64]{2,1,0:T(4,128)(2,1)S(1)} %fusion.126), channel_id=6, replica_groups=mesh['sp'=8,'tp'=4] {'sp'}, dimensions={0}, use_global_device_ids=true | all-gather | bytes 4608 | tf_op jit(solution)/shard_map/all_gather | solution.py:20
  209.5 24.5 %while.85 = (s32[]{:T(128)}, f32[4,64,64]{2,1,0:T(8,128)S(1)}, f32[4,128,64]{2,1,0:T(8,128)S(1)}, s32[]{:T(128)}, bf16[8,4,64]{2,1,0:T(4,128)(2,1)}, /*index=5*/...) while((s32[]{:T(128)}, f32[4,64,64]{2,1,0:T(8,128)S(1)}, ...), condition=%wide.region_20.21_spmd, body=%wide.region_19.20_spmd.sunk | while | flops 148230 | bytes 761523 | solution.py:37
  234.6 2.3 fusion.63
  241.3 2.6 convolution_multiply_fusion.1
  244.8 1.8 copy.252
  248.5 9.3 %while.87 = (s32[]{:T(128)}, f32[4,128,64]{1,2,0:T(8,128)S(1)}, f32[4,4,64,64]{3,2,1,0:T(8,128)}, f32[4,4,1,128]{3,1,2,0:T(4,128)S(1)}, f32[4,4,64,128]{3,2,1,0:...) while((s32[]{:T(128)}, f32[4,128,64]{1,2,0:T(8,128)S(1)}, ...), condition=%wide.region_7.8_spmd.clone, body=%wide.region_6.7_spmd.clone.sunk | while | flops 50462720 | bytes 925804 | solution.py:78
  248.5 1.9 fusion.178
  250.9 1.9 fusion.178
  253.2 1.9 fusion.178
  255.5 1.9 fusion.178
  257.9 33.7 %all-gather.3 = bf16[32,128,64]{1,2,0:T(8,128)(2,1)} all-gather(bf16[4,128,64]{1,2,0:T(8,128)(2,1)S(1)} %convert_element_type.230), channel_id=5, replica_groups=mesh['sp'=8,'tp'=4] {'sp'}, dimensions={0}, use_global_device_ids=true | all-gather | bytes 589824 | tf_op jit(solution)/shard_map/all_gather | solution.py:20
  294.3 1.9 convolution_multiply_fusion.3
  299.4 12.6 %while.86 = (s32[]{:T(128)}, f32[4,64,64]{2,1,0:T(8,128)S(1)}, f32[4,4,64,64]{3,2,1,0:T(8,128)}, f32[4,4,1,64]{3,1,2,0:T(4,128)S(1)}, f32[4,4,64,64]{3,2,1,0:T(8...) while((s32[]{:T(128)}, f32[4,64,64]{2,1,0:T(8,128)S(1)}, ...), condition=%wide.region_2.3_spmd.clone, body=%wide.region_1.2_spmd.clone.sunk | while | flops 25231364 | bytes 792684 | solution.py:78
  302.5 1.8 fusion.173
  305.7 1.8 fusion.173
  308.8 1.8 fusion.173
  312.0 33.2 %all-gather.1 = bf16[32,64,64]{2,1,0:T(8,128)(2,1)} all-gather(bf16[4,64,64]{2,1,0:T(8,128)(2,1)S(1)} %convert_element_type.225), channel_id=3, replica_groups=mesh['sp'=8,'tp'=4] {'sp'}, dimensions={0}, use_global_device_ids=true | all-gather | bytes 294912 | tf_op jit(solution)/shard_map/all_gather | solution.py:20
  345.2 16.3 %all-gather.10 = bf16[8,4,128]{2,1,0:T(4,128)(2,1)S(1)} all-gather(bf16[1,4,128]{2,1,0:T(4,128)(2,1)S(1)} %fusion.125), channel_id=4, replica_groups=mesh['sp'=8,'tp'=4] {'sp'}, dimensions={0}, use_global_device_ids=true | all-gather | bytes 9216 | tf_op jit(solution)/shard_map/all_gather | solution.py:20
  361.5 18.3 %all-gather.9 = bf16[8,4,64]{2,1,0:T(4,128)(2,1)S(1)} all-gather(bf16[1,4,64]{2,1,0:T(4,128)(2,1)S(1)} %fusion.124), channel_id=2, replica_groups=mesh['sp'=8,'tp'=4] {'sp'}, dimensions={0}, use_global_device_ids=true | all-gather | bytes 4608 | tf_op jit(solution)/shard_map/all_gather | solution.py:20
  389.0 2.0 fusion.65
  400.5 31.8 %all-gather.16.cloned.1.call-done = bf16[256,2,1024]{2,0,1:T(8,128)(2,1)} async-done(((bf16[256,2,256]{2,0,1:T(8,128)(2,1)}), bf16[256,2,1024]{2,0,1:T(8,128)(2,1)}) %all-gather.16.cloned.1.call-update) | async-done | bytes 1048592 | tf_op jit(solution)/shard_map/all_gather | solution.py:249
  432.3 6.4 %multiply_reduce_fusion = (f32[256]{0:T(256)S(1)}, f32[256,2048]{1,0:T(8,128)S(1)}) fusion(bf16[256,2,1024]{2,0,1:T(8,128)(2,1)} %all-gather.16.cloned.1.call-done, bf16[2,1024,2048]{2,1,0:T(8,128)(2,1)} %param.41, bf16[256,2048]{1,0:T(8,128)(2,1)} %param.30), kind=kOutput, calls=%fused_computation.86 | convolution fusion | flops 2149580544 | bytes 12583936 | tf_op jit(solution)/shard_map/tgc,gcd->td/dot_general | solution.py:247
  440.4 31.5 %all_to_all.10 = bf16[8,32,2048]{2,1,0:T(8,128)(2,1)} all-to-all(bf16[8,32,2048]{2,1,0:T(8,128)(2,1)S(1)} %bitcast.387), channel_id=1, replica_groups=mesh['sp'=8,'tp'=4] {'sp'}, dimensions={0} | all-to-all | bytes 2097152 | tf_op jit(solution)/shard_map/all_to_all | solution.py:277
  472.1 32.7 %all-gather.18.cloned.1.call-done = bf16[32,32,2048]{2,1,0:T(8,128)(2,1)} async-done(((bf16[8,32,2048]{2,1,0:T(8,128)(2,1)}), bf16[32,32,2048]{2,1,0:T(8,128)(2,1)}) %all-gather.18.cloned.1.call-update) | async-done | bytes 4194320 | tf_op jit(solution)/shard_map/all_gather | solution.py:276
  504.7 7.6 %fusion.50 = f32[4,8,32,1024]{3,2,1,0:T(8,128)S(1)} fusion(bf16[4,8,32,2048]{3,2,1,0:T(8,128)(2,1)} %bitcast.422, bf16[1,2048,1024]{2,1,0:T(8,128)(2,1)} %param.44), kind=kOutput, calls=%fused_computation.74 | convolution fusion | flops 4294967296 | bytes 12582912 | tf_op jit(solution)/shard_map/...d,df->...f/dot_general | solution.py:285
  512.4 5.4 multiply_convert_fusion
  517.8 6.1 fusion.56
  523.9 44.7 %reduce-scatter.2.cloned.1.call-done = bf16[256,2048]{1,0:T(8,128)(2,1)} async-done(((bf16[1024,2048]{1,0:T(8,128)(2,1)}), bf16[256,2048]{1,0:T(8,128)(2,1)}) %reduce-scatter.2.cloned.1.call-update) | async-done | bytes 1048592 | tf_op jit(solution)/shard_map/reduce_scatter | solution.py:290
  568.6 5.8 all-to-all-start.1
  575.0 25.1 %all-to-all-done.1 = bf16[8,32,2048]{2,1,0:T(8,128)(2,1)S(1)} async-done(((bf16[8,32,2048]{2,1,0:T(8,128)(2,1)}), bf16[8,32,2048]{2,1,0:T(8,128)(2,1)S(1)}, u32[]{:S(2)}, u32[]{:S(2)}) %all-to-all-start.1) | async-done | bytes 1048608 | tf_op jit(solution)/shard_map/all_to_all | solution.py:297
  (289 shorter events, 136.7 us)
Async XLA Ops:
  6.5 425.8 %all-gather.16.cloned.1.call-start = ((), (), s32[]{:S(2)}) async-start(), calls=%async_computation.3 | async-start | bytes 1310720 | tf_op jit(solution)/shard_map/all_gather | solution.py:249
  11.1 5.8 copy-start.13
  11.1 6.1 copy-start.24
  42.0 56.2 %copy-start.11 = (f32[256,4,64]{0,2,1:T(8,128)S(1)}, f32[256,4,64]{0,2,1:T(8,128)}, u32[]{:S(2)}) copy-start(f32[256,4,64]{0,2,1:T(8,128)} %get-tuple-element.792) | copy-start | bytes 786436
  106.0 10.7 %copy-start = (f32[4,64,4,64]{3,1,2,0:T(8,128)}, f32[4,64,4,64]{3,1,2,0:T(8,128)S(1)}, u32[]{:S(2)}) copy-start(f32[4,64,4,64]{3,1,2,0:T(8,128)S(1)} %copy.262) | copy-start | bytes 786436
  106.0 6.0 copy-start.5
  106.0 6.0 copy-start.14
  136.1 73.3 %copy-start.4 = (f32[4,4,64,64]{3,2,1,0:T(8,128)}, f32[4,4,64,64]{3,2,1,0:T(8,128)S(1)}, u32[]{:S(2)}) copy-start(f32[4,4,64,64]{3,2,1,0:T(8,128)S(1)} %get-tuple-element.1273) | copy-start | bytes 786436
  209.4 24.6 %copy-start.18 = (f32[4,4,1,128]{3,2,1,0:T(1,128)S(1)}, f32[4,4,1,128]{3,2,1,0:T(1,128)}, u32[]{:S(2)}) copy-start(f32[4,4,1,128]{3,2,1,0:T(1,128)} %reduce-window_subtract_fusion) | copy-start | bytes 24580
  234.0 4.5 copy-start.2
  248.5 45.8 %copy-start.12 = (f32[64,64]{1,0:T(8,128)S(1)}, f32[64,64]{1,0:T(8,128)}, u32[]{:S(2)}) copy-start(f32[64,64]{1,0:T(8,128)} %fusion.121) | copy-start | bytes 49156
  297.3 47.9 %copy-start.22 = (f32[4,128]{1,0:T(4,128)S(1)}, f32[4,128]{1,0:T(4,128)}, u32[]{:S(2)}) copy-start(f32[4,128]{1,0:T(4,128)} %get-tuple-element.798) | copy-start | bytes 6148
  297.3 64.2 %copy-start.23 = (f32[4,64]{1,0:T(4,128)S(1)}, f32[4,64]{1,0:T(4,128)}, u32[]{:S(2)}) copy-start(f32[4,64]{1,0:T(4,128)} %get-tuple-element.803) | copy-start | bytes 3076
  298.5 82.0 %copy-start.7 = (bf16[4,64,4,64]{3,1,2,0:T(8,128)(2,1)}, bf16[4,64,4,64]{3,1,2,0:T(8,128)(2,1)S(1)}, u32[]{:S(2)}) copy-start(bf16[4,64,4,64]{3,1,2,0:T(8,128)(2,1)S(1)} %copy.242) | copy-start | bytes 393220
  380.5 1.7 copy-start.15
  380.5 7.9 %copy-start.1 = (f32[4,64,4,64]{3,1,2,0:T(8,128)S(1)}, f32[4,64,4,64]{3,1,2,0:T(8,128)}, u32[]{:S(2)}) copy-start(f32[4,64,4,64]{3,1,2,0:T(8,128)} %copy-done) | copy-start | bytes 786436
  380.5 7.9 %copy-start.3 = (f32[4,64,64]{2,1,0:T(8,128)S(1)}, f32[4,64,64]{2,1,0:T(8,128)}, u32[]{:S(2)}) copy-start(f32[4,64,64]{2,1,0:T(8,128)} %copy-done.2) | copy-start | bytes 196612
  380.5 7.9 %copy-start.17 = (f32[4,4,1,64]{3,2,1,0:T(1,128)S(1)}, f32[4,4,1,64]{3,2,1,0:T(1,128)}, u32[]{:S(2)}) copy-start(f32[4,4,1,64]{3,2,1,0:T(1,128)} %reduce-window_subtract_fusion.2) | copy-start | bytes 12292
  384.9 6.9 %copy-start.8 = (bf16[4,64,4,64]{3,1,2,0:T(8,128)(2,1)S(1)}, bf16[4,64,4,64]{3,1,2,0:T(8,128)(2,1)}, u32[]{:S(2)}) copy-start(bf16[4,64,4,64]{3,1,2,0:T(8,128)(2,1)} %copy-done.7) | copy-start | bytes 393220
  384.9 6.9 %copy-start.9 = (f32[4,4,64,64]{3,2,1,0:T(8,128)S(1)}, f32[4,4,64,64]{3,2,1,0:T(8,128)}, u32[]{:S(2)}) copy-start(f32[4,4,64,64]{3,2,1,0:T(8,128)} %get-tuple-element.358) | copy-start | bytes 786436
  388.4 5.0 copy-start.16
  391.9 5.5 copy-start.10
  391.9 5.5 copy-start.19
  391.9 5.5 copy-start.26
  393.4 5.6 copy-start.21
  398.6 106.1 %all-gather.18.cloned.1.call-start = ((), (), s32[]{:S(2)}) async-start(), calls=%async_computation.5 | async-start | bytes 5242880 | tf_op jit(solution)/shard_map/all_gather | solution.py:276
  400.4 38.2 %copy-start.20 = (f32[2048]{0:T(1024)S(1)}, f32[2048]{0:T(1024)}, u32[]{:S(2)}) copy-start(f32[2048]{0:T(1024)} %param.42) | copy-start | bytes 24580
  438.7 1.3 copy-start.6
  472.0 96.6 %reduce-scatter.2.cloned.1.call-start = ((), (), s32[]{:S(2)}) async-start(), calls=%async_computation.4 | async-start | bytes 5242880 | tf_op jit(solution)/shard_map/reduce_scatter | solution.py:290
  504.7 7.7 %copy-start.27 = (bf16[1,2048,1024]{2,1,0:T(8,128)(2,1)S(1)}, bf16[1,2048,1024]{2,1,0:T(8,128)(2,1)}, u32[]{:S(2)}) copy-start(bf16[1,2048,1024]{2,1,0:T(8,128)(2,1)} %param.43) | copy-start | bytes 12582916
  504.7 7.7 %copy-start.29 = (bf16[32,32,2048]{2,1,0:T(8,128)(2,1)S(1)}, bf16[32,32,2048]{2,1,0:T(8,128)(2,1)}, u32[]{:S(2)}) copy-start(bf16[32,32,2048]{2,1,0:T(8,128)(2,1)} %all-gather.18.cloned.1.call-done) | copy-start | bytes 12582916
  512.4 5.4 copy-start.28
  523.9 50.9 %copy-start.25 = (f32[256,2]{0,1:T(2,128)S(1)}, f32[256,2]{0,1:T(2,128)}, u32[]{:S(2)}) copy-start(f32[256,2]{0,1:T(2,128)} %param.47) | copy-start | bytes 6148
  568.6 31.5 %all-to-all-start.1 = ((bf16[8,32,2048]{2,1,0:T(8,128)(2,1)}), bf16[8,32,2048]{2,1,0:T(8,128)(2,1)S(1)}, u32[]{:S(2)}, u32[]{:S(2)}) async-start(bf16[8,32,2048]{2,1,0:T(8,128)(2,1)} %bitcast.402), calls=%async_computation.2 | async-start | bytes 2097152 | tf_op jit(solution)/shard_map/all_to_all | solution.py:297
Sparse Core Ops, SparseCore 0:
  398.8 33.4 all-gather.15
  472.1 32.5 all-gather.17
  524.0 44.5 reduce-scatter.1
where the time goes:
time: 621 us; the launch traced here: 612 us
  blocking collectives  240 us (39%)
  waiting for transfers between devices  134 us (22%)
  matrix products  94.5 us (15%)
  local copies, waits for them, and re-layouts  78.4 us (13%)
  other arithmetic  43 us (7%)
  between operations  14.5 us (2%)
    all_gather x8, blocking collectives, entering_2(): lax.all_gather(a.astype(kind), axis)  209 us
    reduce_scatter x1, waiting for transfers between devices, local(): lax.psum_scatter(jnp.dot(flattened, down_weights, preferred_element_type=...  44.7 us
    all_gather x1, waiting for transfers between devices, local(): lax.all_gather(lax.all_to_all(own_buffer, 'sp', split_axis=0, concat_axis...  32.7 us
    all_gather x1, waiting for transfers between devices, local(): lax.all_gather(mixed, 'tp', axis=2, tiled=True)  31.8 us
    all_to_all x1, blocking collectives, local(): lax.all_to_all(own_buffer, 'sp', split_axis=0, concat_axis=0, tiled=True)  31.5 us
    dot_general x16, matrix products, advance(): jnp.einsum('ifm,imo->ifo', block_of_queries, present_state, precision=TOP...  29.8 us
    all_to_all x1, waiting for transfers between devices, local(): lax.all_to_all(returning, 'sp', split_axis=0, concat_axis=0, tiled=True)  25.1 us
    dot_general x16, matrix products, advance(): jnp.einsum('lbi,lbp->lip', block_opening_state, block_of_values, precisio...  16.7 us
  transfers between devices with their start and end apart: 4, of which 4 were waited for; matrix products, arithmetic and copies ran while one was open for 0% of the time, Pallas kernels for 0%

commit v1 on v0

v1 whole, which is shorter than its diff:
```python
from functools import partial

import jax
import jax.numpy as jnp
from jax import lax
from jax.experimental import pallas as pl
from jax.experimental.pallas import tpu as pltpu
from jax.sharding import PartitionSpec as P

BLOCK = 64
LANES = 128
EPS = 1e-06
F32 = jnp.float32
BF16 = jnp.bfloat16
MESH = pl.DeviceIdType.MESH
NT = (((1,), (1,)), ((), ()))
TN = (((0,), (0,)), ((), ()))
VMEM = pl.BlockSpec(memory_space=pltpu.VMEM)


def dot(a, b, dims=(((1,), (0,)), ((), ()))):
    return lax.dot_general(a, b, dims, preferred_element_type=F32)


def split_dot(exact, x):
    hi = x.astype(BF16)
    lo = (x - hi.astype(F32)).astype(BF16)
    return dot(exact, hi) + dot(exact, lo)


def tile_list(narrow, wide, heads, value_size):
    tiles = []
    pairs = heads * value_size // LANES
    for j in range(narrow // LANES):
        tiles.append((0, j * LANES, j * LANES, (2 * j, 2 * j + 1), j * LANES, 2))
    for h in range(wide // LANES):
        at = h * LANES
        tiles.append((1, at, narrow + at, (h, h), (pairs + h // 2) * LANES, h % 2))
    return tiles


def state_mask(kind, value_size):
    rows = lax.broadcasted_iota(jnp.int32, (LANES, LANES), 0) // value_size
    cols = lax.broadcasted_iota(jnp.int32, (LANES, LANES), 1) // value_size
    return rows == cols if kind == 2 else rows == kind


def mix_kernel(heads, nq, wq, v, nf, wf, nr, wr, ex, o_ref, run_ref, msg_ref):
    tokens = nq.shape[0]
    value_size = v.shape[1] // (2 * heads)
    blocks = tokens // BLOCK
    row = lax.broadcasted_iota(jnp.int32, (tokens, tokens), 0)
    col = lax.broadcasted_iota(jnp.int32, (tokens, tokens), 1)
    same = (row // BLOCK) == (col // BLOCK)
    wanted = (same & (row >= col), same & (row <= col))
    tri = tuple(jnp.where(w, 1.0, 0.0).astype(BF16) for w in wanted)
    left = lax.broadcasted_iota(jnp.int32, (1, LANES), 1) < value_size
    o_ref[...] = jnp.zeros_like(o_ref)
    for group, at, place, pair, column, kind in tile_list(nq.shape[1], wq.shape[1], heads, value_size):
        q_ref, f_ref, r_ref = ((nq, nf, nr), (wq, wf, wr))[group]
        lanes = slice(at, at + LANES)
        out_lanes = slice(place, place + LANES)
        columns = slice(column, column + LANES)
        q = jax.nn.silu(q_ref[:, lanes].astype(F32))
        first, second = group * heads + pair[0], group * heads + pair[1]
        extra = jnp.where(left, ex[:, first : first + 1], ex[:, second : second + 1])
        values = v[:, columns]
        mask = state_mask(kind, value_size)
        scores = [None, None]
        carried = [None] * blocks
        for d in range(2):
            opening = jax.nn.sigmoid(-f_ref[d, :, lanes].astype(F32)) * r_ref[d : d + 1, lanes]
            decay = jnp.log1p(-opening) + extra
            inside = split_dot(tri[d], decay)
            query = (q * jnp.exp(inside)).astype(BF16)
            key = (opening * jnp.exp(-inside)).astype(BF16)
            for h in range(2 if kind == 2 else 1):
                own = query if kind != 2 else jnp.where(left == (h == 0), query, jnp.zeros_like(query))
                part = jnp.where(wanted[d], dot(own, key, NT), 0.0)
                scores[h] = part if scores[h] is None else scores[h] + part
            state = None
            prefix = jnp.zeros((1, LANES), F32)
            for b in range(blocks) if d == 0 else range(blocks - 1, -1, -1):
                lo = b * BLOCK
                rows = slice(lo, lo + BLOCK)
                edge = lo + BLOCK - 1 if d == 0 else lo
                ending = inside[edge : edge + 1]
                run_ref[d, rows, out_lanes] = (q[rows] * jnp.exp(prefix + inside[rows])).astype(BF16)
                if state is not None:
                    read = dot(query[rows], state.astype(BF16), NT)
                    carried[b] = read if carried[b] is None else carried[b] + read
                closing = (opening[rows] * jnp.exp(ending - inside[rows])).astype(BF16)
                added = jnp.where(mask, dot(values[rows], closing, TN), 0.0)
                state = added if state is None else state * jnp.exp(ending) + added
                prefix = prefix + ending
            msg_ref[d, :value_size, out_lanes] = (state[:value_size] + state[value_size:]).astype(BF16)
            msg_ref[d, value_size:, out_lanes] = jnp.broadcast_to(
                jnp.exp(prefix), (msg_ref.shape[1] - value_size, LANES)
            ).astype(BF16)
        reads = [dot(s.astype(BF16), values) for s in scores if s is not None]
        if kind == 2:
            within = jnp.where(left, reads[0], reads[1])
        else:
            within = jnp.where(left == (kind == 0), reads[0], 0.0)
        for b in range(blocks):
            rows = slice(b * BLOCK, b * BLOCK + BLOCK)
            total = within[rows]
            if carried[b] is not None:
                total = total + carried[b]
            o_ref[rows, columns] += total


def greet(peers):
    barrier = pltpu.get_barrier_semaphore()
    for peer in peers:
        pl.semaphore_signal(barrier, inc=1, device_id=peer, device_id_type=MESH)
    pl.semaphore_wait(barrier, len(peers))


def remote(src, dst, send, recv, peer):
    return pltpu.make_async_remote_copy(
        src_ref=src, dst_ref=dst, send_sem=send, recv_sem=recv, device_id=peer, device_id_type=MESH
    )


def join_kernel(n, heads, narrow, msg, run, o_in, gates, gain, mixed, held, send, recv):
    me = lax.axis_index("sp")
    value_size = gain.shape[1] // (2 * heads)
    greet([{"sp": lax.rem(me + d, n)} for d in range(1, n)])
    sent = []
    for d in range(1, n):
        to = lax.rem(me + d, n)
        way = jnp.where(to > me, 0, 1)
        copy = remote(msg.at[way], held.at[me], send.at[d], recv.at[me], {"sp": to})
        copy.start()
        sent.append(copy)
    for d in range(1, n):
        source = lax.rem(me + d, n)
        remote(msg.at[0], held.at[source], send.at[d], recv.at[source], {"sp": source}).wait_recv()
    channels = msg.shape[2]

    def one(source, state):
        block = held[source].astype(F32)
        return state * block[value_size : value_size + 1] + block[:value_size]

    zero = jnp.zeros((value_size, channels), F32)
    ahead = lax.fori_loop(0, me, one, zero)
    behind = lax.fori_loop(0, n - 1 - me, lambda i, s: one(n - 1 - i, s), zero)
    entering = (ahead.astype(BF16), behind.astype(BF16))
    sums = {}
    for _, _, place, _, column, kind in tile_list(narrow, channels - narrow, heads, value_size):
        lanes = slice(place, place + LANES)
        mask = state_mask(kind, value_size)
        for d in range(2):
            part = entering[d][:, lanes]
            state = jnp.where(mask, jnp.concatenate([part, part], 0), jnp.zeros((LANES, LANES), BF16))
            read = dot(run[d, :, lanes], state, NT)
            sums[column] = read if column not in sums else sums[column] + read
    ones = jnp.where(state_mask(2, value_size), 1.0, 0.0).astype(BF16)
    for column, total in sums.items():
        columns = slice(column, column + LANES)
        o = o_in[:, columns] + total
        square = o * o
        hi = square.astype(BF16)
        lo = (square - hi.astype(F32)).astype(BF16)
        scale = lax.rsqrt((dot(hi, ones) + dot(lo, ones)) / value_size + EPS)
        gate = jax.nn.silu(gates[:, columns].astype(F32))
        mixed[:, columns] = (o * scale * gain[:, columns] * gate).astype(BF16)
    for copy in sent:
        copy.wait_send()


def spread_kernel(n, x, out, send, recv, local):
    me = lax.axis_index("tp")
    own = pltpu.make_async_copy(x.at[me], out.at[me], local)
    own.start()
    greet([{"tp": lax.rem(me + d, n)} for d in range(1, n)])
    sent = []
    for d in range(1, n):
        to = lax.rem(me + d, n)
        copy = remote(x.at[to], out.at[me], send.at[d], recv.at[me], {"tp": to})
        copy.start()
        sent.append(copy)
    for d in range(1, n):
        source = lax.rem(me + d, n)
        remote(x.at[0], out.at[source], send.at[d], recv.at[source], {"tp": source}).wait_recv()
    for copy in sent:
        copy.wait_send()
    own.wait()


def tp_peers(n):
    me = lax.axis_index("tp")
    low = lax.rem(me, 2)
    sibling = me + 1 - 2 * low
    across = [lax.rem(me + 2 * d, n) for d in range(1, n // 2)]
    return me, sibling, across


def dispatch_kernel(ns, nt, own, out, s1, r1, s2, r2, s3, r3, local):
    here = lax.axis_index("sp")
    me, sibling, across = tp_peers(nt)
    mine = pltpu.make_async_copy(own.at[here], out.at[me, here], local)
    mine.start()
    greet(
        [{"sp": lax.rem(here + d, ns)} for d in range(1, ns)]
        + [{"tp": sibling}]
        + [{"tp": a} for a in across]
    )
    sent = []

    def go(copy):
        copy.start()
        sent.append(copy)

    for d in range(1, ns):
        to = lax.rem(here + d, ns)
        go(remote(own.at[to], out.at[me, here], s1.at[d], r1.at[here], {"sp": to}))

    def source_of(d):
        return lax.rem(here + ns - d, ns)

    def forward(d):
        source = source_of(d)
        for k, a in enumerate(across):
            remote(own.at[0], out.at[a, source], s2.at[k, d], r2.at[a, source], {"tp": a}).wait_recv()
            go(remote(out.at[a, source], out.at[a, source], s3.at[k + 1, d], r3.at[a, source], {"tp": sibling}))

    for d in range(ns):
        source = source_of(d)
        slot = out.at[me, source]
        if d == 0:
            mine.wait()
        else:
            remote(own.at[0], slot, s1.at[d], r1.at[source], {"sp": source}).wait_recv()
        for k, a in enumerate(across):
            go(remote(slot, slot, s2.at[k, d], r2.at[me, source], {"tp": a}))
        go(remote(slot, slot, s3.at[0, d], r3.at[me, source], {"tp": sibling}))
        if d:
            forward(d - 1)
    forward(ns - 1)
    for d in range(ns):
        source = source_of(d)
        for k, a in enumerate([me] + across):
            at = a + sibling - me
            remote(own.at[0], out.at[at, source], s3.at[k, d], r3.at[at, source], {"tp": sibling}).wait_recv()
    for copy in sent:
        copy.wait_send()


def collect_kernel(ns, nt, part, out, got1, buf2, got2, buf3, s1, r1, s2, r2, s3, r3):
    here = lax.axis_index("sp")
    me, sibling, across = tp_peers(nt)
    greet(
        [{"sp": lax.rem(here + d, ns)} for d in range(1, ns)]
        + [{"tp": sibling}]
        + [{"tp": a} for a in across]
    )
    sent = []

    def go(copy):
        copy.start()
        sent.append(copy)

    def target_of(d):
        return lax.rem(here + d, ns)

    order = list(range(1, ns)) + [0]
    for d in order:
        to = target_of(d)
        for k, a in enumerate(across + [me]):
            go(remote(part.at[a + sibling - me, to], got1.at[k, d], s1.at[k, d], r1.at[k, d], {"tp": sibling}))

    def first(d):
        to = target_of(d)
        for k, a in enumerate(across + [me]):
            remote(part.at[0, 0], got1.at[k, d], s1.at[k, d], r1.at[k, d], {"tp": sibling}).wait_recv()
            buf2[k, d] = (part[a, to].astype(F32) + got1[k, d].astype(F32)).astype(BF16)

    def second(d):
        for k, a in enumerate(across):
            go(remote(buf2.at[k, d], got2.at[k, d], s2.at[k, d], r2.at[k, d], {"tp": a}))

    def third(d):
        to = target_of(d)
        total = part[me, to].astype(F32) + got1[len(across), d].astype(F32)
        for k, a in enumerate(across):
            remote(part.at[0, 0], got2.at[k, d], s2.at[k, d], r2.at[k, d], {"tp": a}).wait_recv()
            total = total + got2[k, d].astype(F32)
        if d == 0:
            out[here] = total.astype(BF16)
        else:
            buf3[d] = total.astype(BF16)

    def fourth(d):
        if d:
            to = target_of(d)
            go(remote(buf3.at[d], out.at[here], s3.at[d], r3.at[here], {"sp": to}))

    for i in range(ns + 4):
        for lag, stage in ((0, first), (1, second), (3, third), (4, fourth)):
            if 0 <= i - lag < ns:
                stage(order[i - lag])
    for d in range(1, ns):
        source = target_of(d)
        remote(part.at[0, 0], out.at[source], s3.at[d], r3.at[source], {"sp": source}).wait_recv()
    for copy in sent:
        copy.wait_send()


def call(kernel, shapes, scratch, number, *args):
    shapes = [jax.ShapeDtypeStruct(*s) for s in shapes]
    one = len(shapes) == 1
    params = (
        dict(vmem_limit_bytes=48 * 1024 * 1024)
        if number is None
        else dict(vmem_limit_bytes=48 * 1024 * 1024, collective_id=number, has_side_effects=True)
    )
    return pl.pallas_call(
        kernel,
        out_shape=shapes[0] if one else shapes,
        in_specs=[VMEM] * len(args),
        out_specs=VMEM if one else [VMEM] * len(shapes),
        scratch_shapes=scratch,
        compiler_params=pltpu.CompilerParams(**params),
    )(*args)


def slot_table(block_routes, experts, capacity):
    flattened = block_routes.reshape(-1)
    matches = (flattened[:, None] == jnp.arange(experts, dtype=jnp.int32)[None, :]).astype(
        jnp.int32
    )
    earlier = jnp.cumsum(matches, axis=0) - matches
    token_position = jnp.sum(earlier * matches, axis=1)
    return (flattened * capacity + token_position).reshape(block_routes.shape)


def dispatch(block_slots, block_rows, slot_count):
    picks = jnp.sum(
        (block_slots[:, :, None] == jnp.arange(slot_count, dtype=jnp.int32)).astype(jnp.bfloat16),
        axis=1,
    )
    return jnp.einsum("rs,rd->sd", picks, block_rows, preferred_element_type=jnp.float32).astype(
        jnp.bfloat16
    )


def local(
    stream,
    narrow_query_weight,
    wide_query_weight,
    value_rows_heads,
    output_gate_logits,
    narrow_forget_logits,
    wide_forget_logits,
    narrow_forget_headroom,
    wide_forget_headroom,
    extra_log_decay,
    per_head_norm_gain,
    mixer_output_weight,
    feedforward_norm_gain,
    expert_gate_matrix,
    expert_up_matrix,
    expert_down_matrix,
    routes,
    router_scores_chosen,
):
    ns, nt = lax.axis_size("sp"), lax.axis_size("tp")
    token_rows, model_width = stream.shape
    heads = extra_log_decay.shape[2]
    narrow, wide = narrow_query_weight.shape[1], wide_query_weight.shape[1]
    channels = narrow + wide
    value_size = value_rows_heads.shape[2] // heads
    width = 2 * heads * value_size
    sem = pltpu.SemaphoreType.DMA
    o, run, msg = call(
        partial(mix_kernel, heads),
        [
            ((token_rows, width), F32),
            ((2, token_rows, channels), BF16),
            ((2, value_size + 16, channels), BF16),
        ],
        [],
        None,
        narrow_query_weight,
        wide_query_weight,
        value_rows_heads.reshape(token_rows, width),
        narrow_forget_logits,
        wide_forget_logits,
        narrow_forget_headroom,
        wide_forget_headroom,
        extra_log_decay.reshape(token_rows, 2 * heads),
    )
    mixed = call(
        partial(join_kernel, ns, heads, narrow),
        [((token_rows, width), BF16)],
        [pltpu.VMEM((ns,) + msg.shape[1:], BF16), sem((ns,)), sem((ns,))],
        0,
        msg,
        run,
        o,
        output_gate_logits.reshape(token_rows, width),
        jnp.tile(per_head_norm_gain, 2 * heads)[None],
    )
    row_count = token_rows // nt
    spread = call(
        partial(spread_kernel, nt),
        [((nt, row_count, width), BF16)],
        [sem((nt,)), sem((nt,)), sem],
        1,
        mixed.reshape(nt, row_count, width),
    )
    own_mixed = spread.reshape(nt, row_count, 2, -1).transpose(1, 2, 0, 3).reshape(row_count, -1)
    own_index = lax.axis_index("tp")

    def own_part(x):
        return lax.dynamic_slice_in_dim(x, own_index * row_count, row_count, 0)

    projected = jnp.dot(
        own_mixed,
        mixer_output_weight.reshape(-1, model_width),
        preferred_element_type=F32,
    )
    residual = own_part(stream).astype(F32) + projected
    norm_rows = (
        residual
        * lax.rsqrt(jnp.mean(residual * residual, axis=-1, keepdims=True) + EPS)
        * feedforward_norm_gain
    ).astype(BF16)
    top_count = routes.shape[1]
    capacity = max(2, 2 * top_count * row_count // ns)
    slot_count = ns * capacity
    own_slots = slot_table(own_part(routes), ns, capacity)
    own_buffer = dispatch(own_slots, norm_rows, slot_count).reshape(ns, capacity, model_width)
    pairs = nt // 2
    arrived = call(
        partial(dispatch_kernel, ns, nt),
        [((nt, ns, capacity, model_width), BF16)],
        [sem((ns,)), sem((ns,)), sem((pairs, ns)), sem((nt, ns)), sem((pairs, ns)), sem((nt, ns)), sem],
        2,
        own_buffer,
    ).reshape(-1, model_width)
    gate_part = jnp.dot(arrived, expert_gate_matrix[0], preferred_element_type=F32)
    up_part = jnp.dot(arrived, expert_up_matrix[0], preferred_element_type=F32)
    hidden = (jax.nn.silu(gate_part) * up_part).astype(BF16)
    part = jnp.dot(hidden, expert_down_matrix[0], preferred_element_type=F32).astype(BF16)
    block = (pairs, ns, capacity, model_width)
    returned = call(
        partial(collect_kernel, ns, nt),
        [((ns, capacity, model_width), BF16)],
        [pltpu.VMEM(block, BF16)] * 3
        + [pltpu.VMEM(block[1:], BF16)]
        + [sem((pairs, ns))] * 4
        + [sem((ns,))] * 2,
        3,
        part.reshape(nt, ns, capacity, model_width),
    )
    picked = returned.reshape(slot_count, model_width)[own_slots]
    own_logits = own_part(router_scores_chosen)
    weights = jax.nn.sigmoid(own_logits - own_logits[:, ::-1])
    mixed_out = jnp.sum(weights[:, :, None] * picked.astype(F32), axis=1)
    return (residual + mixed_out).astype(BF16)


def solution(mesh):
    placed = (
        P("sp", None),
        P("sp", "tp"),
        P("sp", "tp"),
        P("sp", None, "tp"),
        P("sp", None, "tp"),
        P(None, "sp", "tp"),
        P(None, "sp", "tp"),
        P(None, "tp"),
        P(None, "tp"),
        P("sp", None, "tp"),
        P(),
        P(),
        P(),
        P("sp", None, "tp"),
        P("sp", None, "tp"),
        P("sp", "tp", None),
        P("sp", None),
        P("sp", None),
    )
    return jax.shard_map(
        local, mesh=mesh, in_specs=placed, out_specs=P(("sp", "tp"), None), check_vma=False
    )
```

time: 621 us -> 159 us (0.26); the launches traced: 612 us -> 158 us
  blocking collectives: 240 us -> 0 us
  waiting for transfers between devices: 134 us -> 0 us
  Pallas kernels: 0 us -> 122 us
  matrix products: 94.5 us -> 20.4 us
  local copies, waits for them, and re-layouts: 78.4 us -> 12.5 us
  other arithmetic: 43 us -> 2.97 us
  between operations: 14.5 us -> 0.27 us
    all_gather x8 -> x0, blocking collectives: 209 us -> none  [entering_2(): lax.all_gather(a.astype(kind), axis)]
    pallas_call x0 -> x5, Pallas kernels: none -> 122 us  [call(): pl.pallas_call(kernel, out_shape=shapes[0] if one else shapes, in_specs=[...]
    dot_general x48 -> x4, matrix products: 94 us -> 19.9 us  [the longest x1 5.33 us: local(): jnp.dot(arrived, expert_gate_matrix[0], preferred_element_type=F32)]
    all_gather x2 -> x0, waiting for transfers between devices: 64.5 us -> none  [the longest x1 32.7 us: local(): lax.all_gather(lax.all_to_all(own_buffer, 'sp', split_axis=0, concat_axis...]
    reduce_scatter x1 -> x0, waiting for transfers between devices: 44.7 us -> none  [local(): lax.psum_scatter(jnp.dot(flattened, down_weights, preferred_element_type=...]
    all_to_all x1 -> x0, blocking collectives: 31.5 us -> none  [local(): lax.all_to_all(own_buffer, 'sp', split_axis=0, concat_axis=0, tiled=True)]
    all_to_all x1 -> x0, waiting for transfers between devices: 25.1 us -> none  [local(): lax.all_to_all(returning, 'sp', split_axis=0, concat_axis=0, tiled=True)]
    rev x13 -> x0, local copies, waits for them, and re-layouts: 13.7 us -> none  [the longest x3 5.7 us: local(): jnp.flip(group[1][1], 0)]
  transfers between devices with their start and end apart: 4 -> 0, of which waited for: 4 -> 0; matrix products, arithmetic and copies ran while one was open for 0% -> 0% of each run, Pallas kernels for 0% -> 0%
where the time goes in v1:
time: 159 us; the launch traced here: 158 us
  Pallas kernels  122 us (77%)
  matrix products  20.4 us (13%)
  local copies, waits for them, and re-layouts  12.5 us (8%)
  other arithmetic  2.97 us (2%)
    pallas_call x5, Pallas kernels, call(): pl.pallas_call(kernel, out_shape=shapes[0] if one else shapes, in_specs=[...  122 us
    unnamed x27, local copies, waits for them, and re-layouts  7.99 us
    dot_general x1, matrix products, local(): jnp.dot(arrived, expert_gate_matrix[0], preferred_element_type=F32)  5.33 us
    dot_general x1, matrix products, local(): jnp.dot(own_mixed, mixer_output_weight.reshape(-1, model_width), preferre...  5.09 us
    dot_general x1, matrix products, local(): jnp.dot(hidden, expert_down_matrix[0], preferred_element_type=F32)  5 us
    dot_general x1, matrix products, local(): up_part = jnp.dot(arrived, expert_up_matrix[0], preferred_element_type=F32)  4.5 us

profile of v1, /device:TPU:0, one launch (start us, length us, event | category | flops | bytes accessed | tf_op | source)
XLA Modules:
  0.0 157.8 jit_solution(397873465315400688)
XLA Ops:
  0.0 0.7 copy-done
  0.7 0.1 constant_dynamic-slice_fusion
  0.8 0.1 copy.31
  0.9 0.1 eq.28
  1.0 0.1 fusion.15
  1.1 0.2 reduce_window_sum.11
  1.3 0.2 select_reduce_fusion
  1.4 0.1 reduce_sum.42
  1.6 0.1 copy.30
  1.7 0.1 fusion.14
  1.8 1.0 copy.32
  2.8 0.7 reshape.55
  3.5 0.1 copy.26.ex
  3.6 0.0 copy-start.1
  3.6 1.0 copy-done.1
  4.7 0.9 copy-done.2
  5.6 0.9 copy-done.3
  6.6 0.9 copy-done.4
  7.5 0.7 copy-done.5
  8.2 0.7 copy-done.6
  8.8 7.1 %shard_map.172 = (f32[256,512]{1,0:T(8,128)S(1)}, bf16[2,256,768]{2,1,0:T(8,128)(2,1)S(1)}, bf16[2,80,768]{2,1,0:T(8,128)(2,1)S(1)}) custom-call(bf16[256,256]{1,0:T(8,128)(2,1)S(1)} %copy-done.4, bf16[256,512]{1,0:T(8,128)(2,1)S(1)} %copy-done.2, bf16[256,512]{1,0:T(8,128)(2,1)S(1)} %bitcast.41, bf16[2,256,256]{2,1,0:T(8,128)(2,1)S(1)} %copy-done.3, ...), custom_call_target="tpu_custom_call" | custom-call | tf_op jit(solution)/shard_map/pallas_call | solution.py:319
  15.9 1.0 copy.33
  16.9 0.7 tile.2
  17.6 0.1 broadcast_in_dim_tile.3.gain
  17.7 22.0 %shard_map.173 = bf16[256,512]{1,0:T(8,128)(2,1)S(1)} custom-call(bf16[2,80,768]{2,1,0:T(8,128)(2,1)S(1)} %get-tuple-element.8.msg, bf16[2,256,768]{2,1,0:T(8,128)(2,1)S(1)} %get-tuple-element.9.run, f32[256,512]{1,0:T(8,128)S(1)} %get-tuple-element.10.o_in, bf16[256,512]{1,0:T(8,128)(2,1)S(1)} %bitcast.39, f32[1,512]{1,0:T(1,128)S(1)} %broadcast_in_dim_tile.3.gain), custom_call_target="tpu_custom_call" | custom-call | tf_op jit(solution)/shard_map/pallas_call | solution.py:319
  39.7 5.2 %shard_map.174 = bf16[4,64,512]{2,1,0:T(8,128)(2,1)S(1)} custom-call(bf16[4,64,512]{2,1,0:T(8,128)(2,1)S(1)} %bitcast.40), custom_call_target="tpu_custom_call" | custom-call | tf_op jit(solution)/shard_map/pallas_call | solution.py:319
  44.8 0.1 reshape.58
  44.9 0.3 copy.35
  45.2 0.2 reshape.59
  45.4 0.0 copy-start.7
  45.4 5.1 %multiply_reduce_fusion.1 = (f32[64]{0:T(128)S(1)}, f32[64,2048]{1,0:T(8,128)S(1)}) fusion(bf16[64,2048]{1,0:T(8,128)(2,1)S(1)} %reshape.59, bf16[2048,2048]{1,0:T(8,128)(2,1)} %bitcast.42, bf16[256,2048]{1,0:T(8,128)(2,1)} %param.18, s32[]{:T(128)S(6)} %select_n.8), kind=kOutput, calls=%fused_computation.14 | convolution fusion | flops 537395136 | bytes 9437444 | tf_op jit(solution)/shard_map/dot_general | solution.py:420
  50.5 0.0 copy-start.9
  50.6 0.5 convolution_convert_fusion
  51.1 45.1 %shard_map.175 = bf16[4,8,32,2048]{3,2,1,0:T(8,128)(2,1)S(1)} custom-call(bf16[8,32,2048]{2,1,0:T(8,128)(2,1)S(1)} %bitcast.38), custom_call_target="tpu_custom_call" | custom-call | tf_op jit(solution)/shard_map/pallas_call | solution.py:319
  96.2 0.0 copy-start.10
  96.2 4.5 %fusion.2 = f32[1024,1024]{1,0:T(8,128)S(1)} fusion(bf16[1024,2048]{1,0:T(8,128)(2,1)S(1)} %bitcast.35, bf16[1,2048,1024]{2,1,0:T(8,128)(2,1)S(1)} %copy-done.9), kind=kOutput, calls=%fused_computation.3 | convolution fusion | flops 4294967296 | bytes 12582912 | tf_op jit(solution)/shard_map/dot_general | solution.py:445
  100.7 0.0 copy-start.11
  100.7 5.3 %multiply_convert_fusion = bf16[1024,1024]{1,0:T(8,128)(2,1)S(1)} fusion(f32[1024,1024]{1,0:T(8,128)S(1)} %fusion.2, bf16[1024,2048]{1,0:T(8,128)(2,1)S(1)} %bitcast.36, bf16[1,2048,1024]{2,1,0:T(8,128)(2,1)S(1)} %copy-done.10), kind=kOutput, calls=%fused_computation.7 | convolution fusion | flops 4301258752 | bytes 14680064 | tf_op jit(solution)/shard_map/dot_general | solution.py:444
  106.1 5.0 %fusion.6 = bf16[1024,2048]{1,0:T(8,128)(2,1)S(1)} fusion(bf16[1024,1024]{1,0:T(8,128)(2,1)S(1)} %multiply_convert_fusion, bf16[1,1024,2048]{2,1,0:T(8,128)(2,1)S(1)} %copy-done.11), kind=kOutput, calls=%fused_computation.8 | convolution fusion | flops 4297064448 | bytes 10485760 | tf_op jit(solution)/shard_map/dot_general | solution.py:447
  111.1 42.3 %shard_map.176 = bf16[8,32,2048]{2,1,0:T(8,128)(2,1)S(1)} custom-call(bf16[4,8,32,2048]{3,2,1,0:T(8,128)(2,1)S(1)} %bitcast.37), custom_call_target="tpu_custom_call" | custom-call | tf_op jit(solution)/shard_map/pallas_call | solution.py:319
  153.4 0.1 reshape.67
  153.5 0.9 gather_fusion
  154.5 0.7 reshape.75
  155.1 0.1 constant_dynamic-slice_fusion.1
  155.2 0.1 add_divide_fusion
  155.3 0.1 copy.28
  155.4 1.6 multiply_reduce_fusion
  157.0 0.8 add_convert_fusion
  (16 shorter events, 0.1 us)
Async XLA Ops:
  0.0 0.7 copy-start
  3.6 1.0 copy-start.1
  4.7 0.9 copy-start.2
  5.6 0.9 copy-start.3
  6.6 0.9 copy-start.4
  7.5 0.7 copy-start.5
  8.1 0.7 copy-start.6
  45.4 5.1 %copy-start.7 = (f32[2048]{0:T(1024)S(1)}, f32[2048]{0:T(1024)}, u32[]{:S(2)}) copy-start(f32[2048]{0:T(1024)} %param.30) | copy-start | bytes 24580
  50.5 45.6 %copy-start.9 = (bf16[1,2048,1024]{2,1,0:T(8,128)(2,1)S(1)}, bf16[1,2048,1024]{2,1,0:T(8,128)(2,1)}, u32[]{:S(2)}) copy-start(bf16[1,2048,1024]{2,1,0:T(8,128)(2,1)} %param.32) | copy-start | bytes 12582916
  96.2 4.5 %copy-start.10 = (bf16[1,2048,1024]{2,1,0:T(8,128)(2,1)S(1)}, bf16[1,2048,1024]{2,1,0:T(8,128)(2,1)}, u32[]{:S(2)}) copy-start(bf16[1,2048,1024]{2,1,0:T(8,128)(2,1)} %param.31) | copy-start | bytes 12582916
  100.7 5.3 %copy-start.11 = (bf16[1,1024,2048]{2,1,0:T(8,128)(2,1)S(1)}, bf16[1,1024,2048]{2,1,0:T(8,128)(2,1)}, u32[]{:S(2)}) copy-start(bf16[1,1024,2048]{2,1,0:T(8,128)(2,1)} %param.33) | copy-start | bytes 12582916
  153.4 1.8 %copy-start.8 = (f32[256,2]{0,1:T(2,128)S(1)}, f32[256,2]{0,1:T(2,128)}, u32[]{:S(2)}) copy-start(f32[256,2]{0,1:T(2,128)} %param.35) | copy-start | bytes 6148

commit v2 on v1

--- a/solution.py
+++ b/solution.py
@@ -110,6 +110,16 @@
             o_ref[rows, columns] += total
 
 
+def partner(me, d, n):
+    assert n & (n - 1) == 0
+    place, bit = me, 1
+    while bit < n:
+        if d & bit:
+            place = place + bit * (1 - 2 * lax.rem(lax.div(me, bit), 2))
+        bit *= 2
+    return place
+
+
 def greet(peers):
     barrier = pltpu.get_barrier_semaphore()
     for peer in peers:
@@ -126,16 +136,16 @@
 def join_kernel(n, heads, narrow, msg, run, o_in, gates, gain, mixed, held, send, recv):
     me = lax.axis_index("sp")
     value_size = gain.shape[1] // (2 * heads)
-    greet([{"sp": lax.rem(me + d, n)} for d in range(1, n)])
+    greet([{"sp": partner(me, d, n)} for d in range(1, n)])
     sent = []
     for d in range(1, n):
-        to = lax.rem(me + d, n)
+        to = partner(me, d, n)
         way = jnp.where(to > me, 0, 1)
         copy = remote(msg.at[way], held.at[me], send.at[d], recv.at[me], {"sp": to})
         copy.start()
         sent.append(copy)
     for d in range(1, n):
-        source = lax.rem(me + d, n)
+        source = partner(me, d, n)
         remote(msg.at[0], held.at[source], send.at[d], recv.at[source], {"sp": source}).wait_recv()
     channels = msg.shape[2]
 
@@ -203,7 +213,7 @@
     mine = pltpu.make_async_copy(own.at[here], out.at[me, here], local)
     mine.start()
     greet(
-        [{"sp": lax.rem(here + d, ns)} for d in range(1, ns)]
+        [{"sp": partner(here, d, ns)} for d in range(1, ns)]
         + [{"tp": sibling}]
         + [{"tp": a} for a in across]
     )
@@ -214,11 +224,11 @@
         sent.append(copy)
 
     for d in range(1, ns):
-        to = lax.rem(here + d, ns)
+        to = partner(here, d, ns)
         go(remote(own.at[to], out.at[me, here], s1.at[d], r1.at[here], {"sp": to}))
 
     def source_of(d):
-        return lax.rem(here + ns - d, ns)
+        return partner(here, d, ns)
 
     def forward(d):
         source = source_of(d)
@@ -252,7 +262,7 @@
     here = lax.axis_index("sp")
     me, sibling, across = tp_peers(nt)
     greet(
-        [{"sp": lax.rem(here + d, ns)} for d in range(1, ns)]
+        [{"sp": partner(here, d, ns)} for d in range(1, ns)]
         + [{"tp": sibling}]
         + [{"tp": a} for a in across]
     )
@@ -263,9 +273,9 @@
         sent.append(copy)
 
     def target_of(d):
-        return lax.rem(here + d, ns)
-
-    order = list(range(1, ns)) + [0]
+        return partner(here, d, ns)
+
+    order = list(range(ns - 1, -1, -1))
     for d in order:
         to = target_of(d)
         for k, a in enumerate(across + [me]):

time: 159 us -> 149 us (0.937)
  Pallas kernels: 122 us -> 112 us
    pallas_call x5, Pallas kernels: 122 us -> 112 us  [call(): pl.pallas_call(kernel, out_shape=shapes[0] if one else shapes, in_specs=[...]
where the time goes in v2:
time: 149 us
  Pallas kernels  112 us (75%)
  matrix products  20.4 us (14%)
  local copies, waits for them, and re-layouts  12.5 us (8%)
  other arithmetic  2.97 us (2%)
    pallas_call x5, Pallas kernels, call(): pl.pallas_call(kernel, out_shape=shapes[0] if one else shapes, in_specs=[...  112 us
    unnamed x27, local copies, waits for them, and re-layouts  7.99 us
    dot_general x1, matrix products, local(): jnp.dot(arrived, expert_gate_matrix[0], preferred_element_type=F32)  5.33 us
    dot_general x1, matrix products, local(): jnp.dot(own_mixed, mixer_output_weight.reshape(-1, model_width), preferre...  5.09 us
    dot_general x1, matrix products, local(): jnp.dot(hidden, expert_down_matrix[0], preferred_element_type=F32)  5.01 us
    dot_general x1, matrix products, local(): up_part = jnp.dot(arrived, expert_up_matrix[0], preferred_element_type=F32)  4.5 us

profile of v2, /device:TPU:0, one launch (start us, length us, event | category | flops | bytes accessed | tf_op | source)
XLA Modules:
  0.0 148.5 jit_solution(4048678149410658613)
XLA Ops:
  0.0 0.7 copy-done
  0.7 0.1 constant_dynamic-slice_fusion
  0.8 0.1 copy.31
  0.9 0.1 eq.28
  1.0 0.1 fusion.15
  1.1 0.2 reduce_window_sum.11
  1.3 0.2 select_reduce_fusion
  1.4 0.1 reduce_sum.42
  1.6 0.1 copy.30
  1.7 0.1 fusion.14
  1.8 1.0 copy.32
  2.8 0.7 reshape.55
  3.5 0.1 copy.26.ex
  3.6 0.0 copy-start.1
  3.6 1.0 copy-done.1
  4.7 0.9 copy-done.2
  5.6 0.9 copy-done.3
  6.6 0.9 copy-done.4
  7.5 0.7 copy-done.5
  8.2 0.7 copy-done.6
  8.8 7.1 %shard_map.172 = (f32[256,512]{1,0:T(8,128)S(1)}, bf16[2,256,768]{2,1,0:T(8,128)(2,1)S(1)}, bf16[2,80,768]{2,1,0:T(8,128)(2,1)S(1)}) custom-call(bf16[256,256]{1,0:T(8,128)(2,1)S(1)} %copy-done.4, bf16[256,512]{1,0:T(8,128)(2,1)S(1)} %copy-done.2, bf16[256,512]{1,0:T(8,128)(2,1)S(1)} %bitcast.41, bf16[2,256,256]{2,1,0:T(8,128)(2,1)S(1)} %copy-done.3, ...), custom_call_target="tpu_custom_call" | custom-call | tf_op jit(solution)/shard_map/pallas_call | solution.py:329
  15.9 1.0 copy.33
  16.9 0.7 tile.2
  17.6 0.1 broadcast_in_dim_tile.3.gain
  17.7 25.2 %shard_map.173 = bf16[256,512]{1,0:T(8,128)(2,1)S(1)} custom-call(bf16[2,80,768]{2,1,0:T(8,128)(2,1)S(1)} %get-tuple-element.8.msg, bf16[2,256,768]{2,1,0:T(8,128)(2,1)S(1)} %get-tuple-element.9.run, f32[256,512]{1,0:T(8,128)S(1)} %get-tuple-element.10.o_in, bf16[256,512]{1,0:T(8,128)(2,1)S(1)} %bitcast.39, f32[1,512]{1,0:T(1,128)S(1)} %broadcast_in_dim_tile.3.gain), custom_call_target="tpu_custom_call" | custom-call | tf_op jit(solution)/shard_map/pallas_call | solution.py:329
  42.9 5.2 %shard_map.174 = bf16[4,64,512]{2,1,0:T(8,128)(2,1)S(1)} custom-call(bf16[4,64,512]{2,1,0:T(8,128)(2,1)S(1)} %bitcast.40), custom_call_target="tpu_custom_call" | custom-call | tf_op jit(solution)/shard_map/pallas_call | solution.py:329
  48.1 0.1 reshape.58
  48.1 0.3 copy.35
  48.5 0.2 reshape.59
  48.7 0.0 copy-start.7
  48.7 5.1 %multiply_reduce_fusion.1 = (f32[64]{0:T(128)S(1)}, f32[64,2048]{1,0:T(8,128)S(1)}) fusion(bf16[64,2048]{1,0:T(8,128)(2,1)S(1)} %reshape.59, bf16[2048,2048]{1,0:T(8,128)(2,1)} %bitcast.42, bf16[256,2048]{1,0:T(8,128)(2,1)} %param.18, s32[]{:T(128)S(6)} %select_n.8), kind=kOutput, calls=%fused_computation.14 | convolution fusion | flops 537395136 | bytes 9437444 | tf_op jit(solution)/shard_map/dot_general | solution.py:430
  53.8 0.0 copy-start.9
  53.8 0.5 convolution_convert_fusion
  54.3 38.2 %shard_map.175 = bf16[4,8,32,2048]{3,2,1,0:T(8,128)(2,1)S(1)} custom-call(bf16[8,32,2048]{2,1,0:T(8,128)(2,1)S(1)} %bitcast.38), custom_call_target="tpu_custom_call" | custom-call | tf_op jit(solution)/shard_map/pallas_call | solution.py:329
  92.5 0.0 copy-start.10
  92.6 4.5 %fusion.2 = f32[1024,1024]{1,0:T(8,128)S(1)} fusion(bf16[1024,2048]{1,0:T(8,128)(2,1)S(1)} %bitcast.35, bf16[1,2048,1024]{2,1,0:T(8,128)(2,1)S(1)} %copy-done.9), kind=kOutput, calls=%fused_computation.3 | convolution fusion | flops 4294967296 | bytes 12582912 | tf_op jit(solution)/shard_map/dot_general | solution.py:455
  97.1 0.0 copy-start.11
  97.1 5.3 %multiply_convert_fusion = bf16[1024,1024]{1,0:T(8,128)(2,1)S(1)} fusion(f32[1024,1024]{1,0:T(8,128)S(1)} %fusion.2, bf16[1024,2048]{1,0:T(8,128)(2,1)S(1)} %bitcast.36, bf16[1,2048,1024]{2,1,0:T(8,128)(2,1)S(1)} %copy-done.10), kind=kOutput, calls=%fused_computation.7 | convolution fusion | flops 4301258752 | bytes 14680064 | tf_op jit(solution)/shard_map/dot_general | solution.py:454
  102.4 5.0 %fusion.6 = bf16[1024,2048]{1,0:T(8,128)(2,1)S(1)} fusion(bf16[1024,1024]{1,0:T(8,128)(2,1)S(1)} %multiply_convert_fusion, bf16[1,1024,2048]{2,1,0:T(8,128)(2,1)S(1)} %copy-done.11), kind=kOutput, calls=%fused_computation.8 | convolution fusion | flops 4297064448 | bytes 10485760 | tf_op jit(solution)/shard_map/dot_general | solution.py:457
  107.4 36.7 %shard_map.176 = bf16[8,32,2048]{2,1,0:T(8,128)(2,1)S(1)} custom-call(bf16[4,8,32,2048]{3,2,1,0:T(8,128)(2,1)S(1)} %bitcast.37), custom_call_target="tpu_custom_call" | custom-call | tf_op jit(solution)/shard_map/pallas_call | solution.py:329
  144.1 0.1 reshape.67
  144.3 0.9 gather_fusion
  145.2 0.7 reshape.75
  145.9 0.1 constant_dynamic-slice_fusion.1
  146.0 0.1 add_divide_fusion
  146.1 0.1 copy.28
  146.2 1.6 %multiply_reduce_fusion = f32[64,2048]{1,0:T(8,128)S(1)} fusion(f32[64,2,2048]{2,1,0:T(2,128)S(1)} %reshape.75, f32[64,2]{1,0:T(8,128)S(1)} %copy.28), kind=kLoop, calls=%fused_computation.11 | loop fusion | flops 393216 | bytes 1573376 | tf_op jit(solution)/shard_map/reduce_sum | solution.py:472
  147.8 0.8 add_convert_fusion
  (16 shorter events, 0.1 us)
Async XLA Ops:
  0.0 0.7 copy-start
  3.6 1.0 copy-start.1
  4.7 0.9 copy-start.2
  5.6 0.9 copy-start.3
  6.6 0.9 copy-start.4
  7.5 0.7 copy-start.5
  8.1 0.7 copy-start.6
  48.7 5.1 %copy-start.7 = (f32[2048]{0:T(1024)S(1)}, f32[2048]{0:T(1024)}, u32[]{:S(2)}) copy-start(f32[2048]{0:T(1024)} %param.30) | copy-start | bytes 24580
  53.8 38.8 %copy-start.9 = (bf16[1,2048,1024]{2,1,0:T(8,128)(2,1)S(1)}, bf16[1,2048,1024]{2,1,0:T(8,128)(2,1)}, u32[]{:S(2)}) copy-start(bf16[1,2048,1024]{2,1,0:T(8,128)(2,1)} %param.32) | copy-start | bytes 12582916
  92.5 4.5 %copy-start.10 = (bf16[1,2048,1024]{2,1,0:T(8,128)(2,1)S(1)}, bf16[1,2048,1024]{2,1,0:T(8,128)(2,1)}, u32[]{:S(2)}) copy-start(bf16[1,2048,1024]{2,1,0:T(8,128)(2,1)} %param.31) | copy-start | bytes 12582916
  97.1 5.3 %copy-start.11 = (bf16[1,1024,2048]{2,1,0:T(8,128)(2,1)S(1)}, bf16[1,1024,2048]{2,1,0:T(8,128)(2,1)}, u32[]{:S(2)}) copy-start(bf16[1,1024,2048]{2,1,0:T(8,128)(2,1)} %param.33) | copy-start | bytes 12582916
  144.1 1.8 %copy-start.8 = (f32[256,2]{0,1:T(2,128)S(1)}, f32[256,2]{0,1:T(2,128)}, u32[]{:S(2)}) copy-start(f32[256,2]{0,1:T(2,128)} %param.35) | copy-start | bytes 6148
